TPU v7x, 512 devices: a whole 4x8x8 slice. The times are simulated.
512 devices in a mesh: sp: 32 (over z, x), tp: 16 (over y, core).
Axes of the slice: x: 4, y: 8, z: 8, core: 2. Of those that a mesh axis runs over, the one named last changes fastest.
Arguments:
- queries: bfloat16 [8192, 1024], P('sp', 'tp'), may hold values from -6 to 6
- keys: bfloat16 [8192, 256], P('sp'), may hold values from -6 to 6
- values: bfloat16 [8192, 256], P('sp'), may hold values from -6 to 6
- sink: float32 [16], P('tp'), may hold values from 3 to 6
- w_out: bfloat16 [1024, 2048], P('tp'), may hold values from -0.1875 to 0.1875
- stream: bfloat16 [8192, 2048], P(('sp', 'tp')), may hold values from -6 to 6
- gain: bfloat16 [2048], replicated, may hold values from 0.099609375 to 1.8984375
- routes: int32 [8192, 4], P('sp'), may hold values from 0 to 63, all different within a row; in each aligned block of 16 rows (0 to 15, 16 to 31, ...) at most 2 rows name the same one
- route_weights: float32 [8192, 4], P('sp'), may hold values from 0.2 to 1
- w_gate: bfloat16 [64, 1024, 2048], P('sp', 'tp'), may hold values from -0.125 to 0.125
- w_up: bfloat16 [64, 1024, 2048], P('sp', 'tp'), may hold values from -0.125 to 0.125
- w_down: bfloat16 [64, 1024, 2048], P('sp', None, 'tp'), may hold values from -0.1875 to 0.1875
- shared_gate: bfloat16 [1024, 2048], P('tp'), may hold values from -0.125 to 0.125
- shared_up: bfloat16 [1024, 2048], P('tp'), may hold values from -0.125 to 0.125
- shared_down: bfloat16 [1024, 2048], P(None, 'tp'), may hold values from -0.1875 to 0.1875
Outputs:
- layer_out: bfloat16 [8192, 2048], P('sp', 'tp')
Inputs may be any that keep to these rules, and one draw needn't show every extreme that they name: `routes`: in each aligned block of 16 rows no expert is named in more than 2 rows, and some blocks reach 2; a row names 4 different experts.
All inputs are finite; a program needn't handle non-finite values.
Results may differ from a plain program's by a relative error of at most 0.014.
Values may be sent and summed in bfloat16 or wider, within the bound.
A program may use at most 64 MiB of HBM per device.

v0:
```python
import jax
import jax.numpy as jnp
from jax import lax
from jax.sharding import PartitionSpec as P

D = 2048
HEADS = 16
KV_HEADS = 4
HD = 64
WINDOW = 128
EXPERTS = 64
TOPK = 4
NORM_EPS = 1e-05


def with_halo(array, sides, width):
    for axis, dim in sides:
        devices, length = (lax.axis_size(axis), array.shape[dim])
        up = [(i, (i + 1) % devices) for i in range(devices - 1)]
        down = [(j, i) for i, j in up]
        last = lax.slice_in_dim(array, length - width, length, axis=dim)
        leading = lax.slice_in_dim(array, 0, width, axis=dim)
        before = lax.ppermute(last, axis, up)
        after = lax.ppermute(leading, axis, down)
        array = jnp.concatenate([before, array, after], axis=dim)
    return array


def laid_out(tiles, dim):
    tiles = jnp.moveaxis(tiles, 0, dim)
    dims = tiles.shape
    return tiles.reshape(*dims[:dim], dims[dim] * dims[dim + 1], *dims[dim + 2 :])


def from_everyone(array, axis):
    copies = jnp.broadcast_to(array, (lax.axis_size(axis), *array.shape))
    return lax.all_to_all(copies, axis, split_axis=0, concat_axis=0, tiled=True)


def gathered_copies(array, axis, dim):
    return laid_out(from_everyone(array, axis), dim)


def taken_together(array, axis):
    return from_everyone(array, axis).sum(axis=0)


def gather_turned(arrays, axis, dims):
    turned = [jnp.moveaxis(a, dim, 0) for a, dim in zip(arrays, dims)]
    widths = [t[0].size for t in turned]
    both = jnp.concatenate([t.reshape(-1, w) for t, w in zip(turned, widths)], axis=1)
    result = lax.all_gather(both, axis, axis=0, tiled=True)
    tiles = jnp.split(result, [sum(widths[:k]) for k in range(1, len(widths))], axis=1)
    return tuple(
        (
            jnp.moveaxis(b.reshape(-1, *t.shape[1:]), 0, dim)
            for b, t, dim in zip(tiles, turned, dims)
        )
    )


def slot_ids(block_routes, capacity):
    flat_routes = block_routes.reshape(-1)
    hit_table = (flat_routes[:, None] == jnp.arange(EXPERTS)[None, :]).astype(jnp.int32)
    earlier = jnp.cumsum(hit_table, axis=0) - hit_table
    slot_rank = jnp.sum(earlier * hit_table, axis=1)
    return flat_routes * capacity + slot_rank


def local(
    queries,
    keys,
    values,
    sink,
    w_out,
    stream,
    gain,
    routes,
    route_weights,
    w_gate,
    w_up,
    w_down,
    shared_gate,
    shared_up,
    shared_down,
):
    tok_dev = queries.shape[0]
    n_tp = lax.axis_size("tp")
    n_sp = lax.axis_size("sp")
    tp_idx = lax.axis_index("tp")
    sp_idx = lax.axis_index("sp")
    heads_dev = HEADS // n_tp
    group = HEADS // KV_HEADS
    kv_head = tp_idx * heads_dev // group
    key_own = lax.dynamic_slice_in_dim(keys, kv_head * HD, HD, 1)
    value_own = lax.dynamic_slice_in_dim(values, kv_head * HD, HD, 1)
    paired = jnp.concatenate([key_own, value_own], axis=1)
    padded = with_halo(paired, (("sp", 0),), WINDOW)
    blocks = tok_dev // WINDOW
    framed = padded.reshape(blocks + 2, WINDOW, 2 * HD)
    banded = jnp.concatenate([framed[:-2], framed[1:-1], framed[2:]], axis=1)
    key_band = banded[:, :, :HD]
    value_band = banded[:, :, HD:]
    query_blocks = queries.reshape(blocks, WINDOW, heads_dev, HD)
    scores = jnp.einsum(
        "nqhd,njd->nhqj", query_blocks, key_band, preferred_element_type=jnp.float32
    ) * HD ** (-0.5)
    offset = sp_idx * tok_dev
    seq_total = tok_dev * n_sp
    query_pos = (
        offset + jnp.arange(blocks)[:, None, None] * WINDOW + jnp.arange(WINDOW)[None, :, None]
    )
    key_pos = (
        offset
        - WINDOW
        + jnp.arange(blocks)[:, None, None] * WINDOW
        + jnp.arange(3 * WINDOW)[None, None, :]
    )
    allowed = (jnp.abs(query_pos - key_pos) <= WINDOW) & (key_pos >= 0) & (key_pos < seq_total)
    scores = jnp.where(allowed[:, None], scores, -jnp.inf)
    sink_level = sink.reshape(1, heads_dev, 1, 1)
    row_peak = jnp.maximum(scores.max(-1, keepdims=True), sink_level)
    probabilities = jnp.exp(scores - row_peak)
    denominator = probabilities.sum(-1, keepdims=True) + jnp.exp(sink_level - row_peak)
    weights = (probabilities / denominator).astype(jnp.bfloat16)
    attended = jnp.einsum("nhqj,njd->nqhd", weights, value_band, preferred_element_type=jnp.float32)
    attended = attended.astype(jnp.bfloat16).reshape(tok_dev, heads_dev * HD)
    rows_dev = tok_dev // n_tp
    d_dev = w_down.shape[2]
    all_heads = gathered_copies(attended, "tp", 1)
    w_cols, stream_cols = (
        lax.all_to_all(w_out, "tp", split_axis=1, concat_axis=0, tiled=True),
        lax.all_to_all(stream, "tp", split_axis=1, concat_axis=0, tiled=True),
    )
    projected = jnp.dot(all_heads, w_cols, preferred_element_type=jnp.float32)
    mixed_cols = (stream_cols.astype(jnp.float32) + projected).astype(jnp.bfloat16)
    residual = mixed_cols.astype(jnp.float32)
    square_sum = taken_together(jnp.sum(residual * residual, axis=-1), "tp")
    scale_rows = lax.rsqrt(square_sum[:, None] / D + NORM_EPS)
    gain_cols = lax.dynamic_slice_in_dim(gain, tp_idx * d_dev, d_dev, 0).astype(jnp.float32)
    normed_cols = (residual * scale_rows * gain_cols[None, :]).astype(jnp.bfloat16)
    normed = gathered_copies(normed_cols, "tp", 1)
    exp_dev = w_gate.shape[0]
    capacity = max(1, 2 * tok_dev * TOPK // (n_tp * EXPERTS))
    slot_count = EXPERTS * capacity
    blocked_routes = routes.reshape(n_tp, rows_dev, TOPK)
    destination = jax.vmap(lambda block_routes: slot_ids(block_routes, capacity))(blocked_routes)
    slot_select = destination[:, None, :] == jnp.arange(slot_count)[None, :, None]
    slot_select = slot_select.reshape(n_tp, slot_count, rows_dev, TOPK).astype(jnp.float32)
    dispatch_table = jnp.sum(slot_select, axis=-1).astype(jnp.bfloat16)
    combine_table = jnp.sum(slot_select * route_weights.reshape(n_tp, 1, rows_dev, TOPK), axis=-1)
    normed_blocks = normed.reshape(n_tp, rows_dev, D)
    own_table = lax.dynamic_index_in_dim(dispatch_table, tp_idx, 0, keepdims=False)
    own_rows = lax.dynamic_index_in_dim(normed_blocks, tp_idx, 0, keepdims=False)
    outgoing = jnp.dot(own_table, own_rows, preferred_element_type=jnp.float32).astype(jnp.bfloat16)
    arrived = lax.all_to_all(outgoing, "sp", split_axis=0, concat_axis=0, tiled=True)
    arrived = arrived.reshape(1, n_sp, exp_dev, capacity, D)
    piece_rows = lax.all_gather(arrived, "tp", axis=0, tiled=True)
    gate_act = jnp.einsum(
        "tsecd,efd->tsecf", piece_rows, w_gate, preferred_element_type=jnp.float32
    )
    up_act = jnp.einsum("tsecd,efd->tsecf", piece_rows, w_up, preferred_element_type=jnp.float32)
    hidden = (jax.nn.silu(gate_act) * up_act).astype(jnp.bfloat16)
    shared_gate_act = jnp.einsum(
        "td,fd->tf", normed, shared_gate, preferred_element_type=jnp.float32
    )
    shared_up_act = jnp.einsum("td,fd->tf", normed, shared_up, preferred_element_type=jnp.float32)
    shared_hidden = (jax.nn.silu(shared_gate_act) * shared_up_act).astype(jnp.bfloat16)
    shared_hidden = shared_hidden.reshape(1, 1, 1, tok_dev, shared_hidden.shape[1])
    expert_piece, shared_piece = gather_turned((hidden, shared_hidden), "tp", (4, 4))
    piece_width = expert_piece.shape[4]
    routed_total = jnp.einsum(
        "tsecf,efd->tsecd", expert_piece, w_down, preferred_element_type=jnp.float32
    )
    shared_total = jnp.dot(
        shared_piece.reshape(tok_dev, piece_width), shared_down, preferred_element_type=jnp.float32
    )
    returned = lax.all_to_all(
        routed_total.astype(jnp.bfloat16), "sp", split_axis=1, concat_axis=1, tiled=True
    )
    returned = returned.reshape(n_tp, slot_count, d_dev).astype(jnp.float32)
    routed = jnp.einsum("tmr,tmd->trd", combine_table, returned)
    routed = routed.reshape(tok_dev, d_dev)
    return (residual + routed + shared_total).astype(jnp.bfloat16)


def solution(mesh):
    placed = (
        P("sp", "tp"),
        P("sp", None),
        P("sp", None),
        P("tp"),
        P("tp", None),
        P(("sp", "tp"), None),
        P(),
        P("sp", None),
        P("sp", None),
        P("sp", "tp", None),
        P("sp", "tp", None),
        P("sp", None, "tp"),
        P("tp", None),
        P("tp", None),
        P(None, "tp"),
    )
    return jax.shard_map(
        local, mesh=mesh, in_specs=placed, out_specs=P("sp", "tp"), check_vma=False
    )
```

profile of v0, /device:TPU:8, one launch (start us, length us, event | category | flops | bytes accessed | tf_op | source)
XLA Modules:
  0.0 313.8 jit_solution(5770819059560762188)
XLA Ops:
  6.5 1.5 copy_bitcast_fusion.1
  8.1 9.1 %all-to-all-start = ((bf16[16,16,128]{2,0,1:T(8,128)(2,1)}), bf16[16,16,128]{2,0,1:T(8,128)(2,1)S(1)}, u32[]{:S(2)}, u32[]{:S(2)}) async-start(bf16[16,16,128]{2,0,1:T(8,128)(2,1)} %copy_bitcast_fusion.1), calls=%async_computation | async-start | bytes 131072 | tf_op jit(solution)/shard_map/all_to_all | solution.py:133
  17.2 1.0 constant_dynamic-slice_fusion
  18.2 1.9 collective-permute-start
  20.1 1.3 collective-permute-start.1
  21.6 1.7 copy_bitcast_fusion
  24.1 1.9 collective-permute-done.1
  26.5 1.3 fusion.51
  27.8 7.2 %all-to-all-start.2 = ((bf16[64,16,128]{2,0,1:T(8,128)(2,1)}), bf16[64,16,128]{2,0,1:T(8,128)(2,1)S(1)}, u32[]{:S(2)}, u32[]{:S(2)}) async-start(bf16[64,16,128]{2,0,1:T(8,128)(2,1)} %copy_bitcast_fusion), calls=%async_computation.2 | async-start | bytes 524288 | tf_op jit(solution)/shard_map/all_to_all | solution.py:132
  35.2 0.2 fusion.19
  35.4 9.2 %all-to-all-done.2 = bf16[64,16,128]{2,0,1:T(8,128)(2,1)S(1)} async-done(((bf16[64,16,128]{2,0,1:T(8,128)(2,1)}), bf16[64,16,128]{2,0,1:T(8,128)(2,1)S(1)}, u32[]{:S(2)}, u32[]{:S(2)}) %all-to-all-start.2) | async-done | bytes 262176 | tf_op jit(solution)/shard_map/all_to_all | solution.py:132
  44.7 0.8 broadcast_in_dim.11
  45.5 5.0 %all-to-all-start.1 = ((bf16[16,256,64]{1,2,0:T(8,128)(2,1)}), bf16[16,256,64]{1,2,0:T(8,128)(2,1)S(1)}, u32[]{:S(2)}, u32[]{:S(2)}) async-start(bf16[16,256,64]{1,2,0:T(8,128)(2,1)} %broadcast_in_dim.11), calls=%async_computation.1 | async-start | bytes 1048576 | tf_op jit(solution)/shard_map/all_to_all | solution.py:37
  50.7 14.4 %all-to-all-done.1 = bf16[16,256,64]{1,2,0:T(8,128)(2,1)S(1)} async-done(((bf16[16,256,64]{1,2,0:T(8,128)(2,1)}), bf16[16,256,64]{1,2,0:T(8,128)(2,1)S(1)}, u32[]{:S(2)}, u32[]{:S(2)}) %all-to-all-start.1) | async-done | bytes 524320 | tf_op jit(solution)/shard_map/all_to_all | solution.py:37
  65.1 0.3 multiply_reduce_fusion
  65.4 0.6 broadcast_in_dim.12
  66.0 5.7 %all-to-all-start.3 = ((f32[16,1,256]{2,1,0:T(1,128)}), f32[16,1,256]{2,1,0:T(1,128)S(1)}, u32[]{:S(2)}, u32[]{:S(2)}) async-start(f32[16,1,256]{2,1,0:T(1,128)} %broadcast_in_dim.12), calls=%async_computation.3 | async-start | bytes 32768 | tf_op jit(solution)/shard_map/all_to_all | solution.py:37
  71.7 0.8 dynamic-slice_convert_fusion.1
  72.4 5.5 %all-to-all-done.3 = f32[16,1,256]{2,1,0:T(1,128)S(1)} async-done(((f32[16,1,256]{2,1,0:T(1,128)}), f32[16,1,256]{2,1,0:T(1,128)S(1)}, u32[]{:S(2)}, u32[]{:S(2)}) %all-to-all-start.3) | async-done | bytes 16416 | tf_op jit(solution)/shard_map/all_to_all | solution.py:37
  78.1 1.1 broadcast_in_dim.13
  79.2 4.9 %all-to-all-start.4 = ((bf16[16,256,128]{1,2,0:T(8,128)(2,1)}), bf16[16,256,128]{1,2,0:T(8,128)(2,1)S(1)}, u32[]{:S(2)}, u32[]{:S(2)}) async-start(bf16[16,256,128]{1,2,0:T(8,128)(2,1)} %broadcast_in_dim.13), calls=%async_computation.4 | async-start | bytes 2097152 | tf_op jit(solution)/shard_map/all_to_all | solution.py:37
  84.7 1.4 select_reduce_fusion.1
  86.2 1.0 select_reduce_fusion
  87.2 21.5 %all-to-all-done.4 = bf16[16,256,128]{1,2,0:T(8,128)(2,1)S(1)} async-done(((bf16[16,256,128]{1,2,0:T(8,128)(2,1)}), bf16[16,256,128]{1,2,0:T(8,128)(2,1)S(1)}, u32[]{:S(2)}, u32[]{:S(2)}) %all-to-all-start.4) | async-done | bytes 1048608 | tf_op jit(solution)/shard_map/all_to_all | solution.py:37
  108.7 1.1 copy.141
  109.8 1.3 reshape_reshape.2
  111.1 1.2 convolution_convert_fusion
  112.2 0.2 all_to_all.49
  112.4 33.3 %all_to_all.59 = bf16[32,4,2048]{2,1,0:T(4,128)(2,1)S(1)} all-to-all(bf16[32,4,2048]{2,1,0:T(4,128)(2,1)S(1)} %all_to_all.49), channel_id=1, replica_groups=mesh['sp'=32,'tp'=16] {'sp'}, dimensions={0} | all-to-all | bytes 1048576 | tf_op jit(solution)/shard_map/all_to_all | solution.py:156
  145.7 1.1 copy.142
  146.8 0.2 all-gather.5.cloned.1.call-start
  147.1 0.3 fusion.52
  147.4 1.2 fusion.18
  148.8 50.0 %all-gather.3.cloned.1.call-done = bf16[16,32,2,2,2048]{4,1,3,0,2:T(8,128)(2,1)} async-done(((bf16[1,32,2,2,2048]{4,1,3,0,2:T(8,128)(2,1)}), bf16[16,32,2,2,2048]{4,1,3,0,2:T(8,128)(2,1)}) %all-gather.3.cloned.1.call-update) | async-done | bytes 8388624 | tf_op jit(solution)/shard_map/all_gather | solution.py:158
  198.8 5.8 %convolution_bitcast_fusion.1 = f32[64,16,32,2,2]{0,2,4,1,3:T(8,128)S(1)} fusion(bf16[16,32,2,2,2048]{4,1,3,0,2:T(8,128)(2,1)} %all-gather.3.cloned.1.call-done, bf16[2,64,2048]{2,1,0:T(8,128)(2,1)S(1)} %copy-done.2), kind=kOutput, calls=%fused_computation.6 | convolution fusion | flops 536870912 | bytes 9437184 | tf_op jit(solution)/shard_map/tsecd,efd->tsecf/dot_general | solution.py:159
  204.7 2.3 fusion.4
  207.0 0.5 copy.143
  207.6 1.0 copy.145
  208.6 44.9 %all-gather.5.cloned.1.call-done = bf16[1024,2304]{1,0:T(8,128)(2,1)} async-done(((bf16[64,2304]{1,0:T(8,128)(2,1)}), bf16[1024,2304]{1,0:T(8,128)(2,1)}) %all-gather.5.cloned.1.call-update) | async-done | bytes 4718608 | tf_op jit(solution)/shard_map/all_gather | solution.py:52
  253.5 4.8 %split.8 = bf16[1024,2048]{1,0:T(8,128)(2,1)} slice(bf16[1024,2304]{1,0:T(8,128)(2,1)} %all-gather.5.cloned.1.call-done), slice={[0:1024], [0:2048]} | slice | bytes 8388608 | tf_op jit(solution)/shard_map/split | solution.py:53
  258.3 6.5 %copy.146 = bf16[1024,2048]{0,1:T(8,128)(2,1)} copy(bf16[1024,2048]{1,0:T(8,128)(2,1)} %split.8) | data formatting | bytes 8388608 | tf_op jit(solution)/shard_map/split | solution.py:53
  264.8 7.2 %reshape.237 = bf16[1024,16,32,2,2]{0,4,3,2,1:T(2,128)(2,1)} reshape(bf16[1024,2048]{0,1:T(8,128)(2,1)} %copy.146) | data formatting | bytes 8388608 | tf_op jit(solution)/shard_map/reshape | solution.py:56
  272.0 3.6 %fusion.8 = bf16[16,32,2,2,128]{4,1,3,0,2:T(8,128)(2,1)S(1)} fusion(bf16[1024,16,32,2,2]{0,4,3,2,1:T(2,128)(2,1)} %reshape.237, bf16[2,1024,128]{2,1,0:T(8,128)(2,1)S(1)} %copy-done), kind=kOutput, calls=%fused_computation.9 | convolution fusion | flops 537133056 | bytes 5242880 | tf_op jit(solution)/shard_map/tsecf,efd->tsecd/dot_general | solution.py:172
  275.6 0.5 copy.148
  276.2 28.2 %all_to_all.60 = bf16[16,32,2,2,128]{4,3,0,2,1:T(2,128)(2,1)S(1)} all-to-all(bf16[16,32,2,2,128]{4,3,0,2,1:T(2,128)(2,1)S(1)} %copy.148), channel_id=1, replica_groups=mesh['sp'=32,'tp'=16] {'sp'}, dimensions={1} | all-to-all | bytes 1048576 | tf_op jit(solution)/shard_map/all_to_all | solution.py:178
  304.5 0.3 fusion.28
  304.9 1.3 fusion.16
  306.2 0.7 copy.153
  (58 shorter events, 2.4 us)
Async XLA Ops:
  6.5 265.5 %copy-start = (bf16[2,1024,128]{2,1,0:T(8,128)(2,1)S(1)}, bf16[2,1024,128]{2,1,0:T(8,128)(2,1)}, u32[]{:S(2)}) copy-start(bf16[2,1024,128]{2,1,0:T(8,128)(2,1)} %param.26) | copy-start | bytes 1572868
  8.1 19.8 %all-to-all-start = ((bf16[16,16,128]{2,0,1:T(8,128)(2,1)}), bf16[16,16,128]{2,0,1:T(8,128)(2,1)S(1)}, u32[]{:S(2)}, u32[]{:S(2)}) async-start(bf16[16,16,128]{2,0,1:T(8,128)(2,1)} %copy_bitcast_fusion.1), calls=%async_computation | async-start | bytes 131072 | tf_op jit(solution)/shard_map/all_to_all | solution.py:133
  18.2 5.8 %collective-permute-start = (bf16[128,128]{1,0:T(8,128)(2,1)S(1)}, bf16[128,128]{1,0:T(8,128)(2,1)S(1)}, u32[]{:S(2)}, u32[]{:S(2)}) collective-permute-start(bf16[128,128]{1,0:T(8,128)(2,1)S(1)} %get-tuple-element.10), channel_id=1, source_target_pairs={{0,16},{16,32},{32,48},{48,64},{64,80},{80,96},{96,112},{112,128},... | collective-permute-start | bytes 98312 | tf_op jit(solution)/shard_map/ppermute | solution.py:23
  20.1 5.8 %collective-permute-start.1 = (bf16[128,128]{1,0:T(8,128)(2,1)S(1)}, bf16[128,128]{1,0:T(8,128)(2,1)S(1)}, u32[]{:S(2)}, u32[]{:S(2)}) collective-permute-start(bf16[128,128]{1,0:T(8,128)(2,1)S(1)} %get-tuple-element.11), channel_id=1, source_target_pairs={{16,0},{32,16},{48,32},{64,48},{80,64},{96,80},{112,96},{128,112},... | collective-permute-start | bytes 98312 | tf_op jit(solution)/shard_map/ppermute | solution.py:24
  27.8 56.3 %copy-start.6 = (s32[256,4]{0,1:T(4,128)S(1)}, s32[256,4]{0,1:T(4,128)}, u32[]{:S(2)}) copy-start(s32[256,4]{0,1:T(4,128)} %param.22) | copy-start | bytes 12292
  27.8 56.5 %copy-start.7 = (f32[256,4]{0,1:T(4,128)S(1)}, f32[256,4]{0,1:T(4,128)}, u32[]{:S(2)}) copy-start(f32[256,4]{0,1:T(4,128)} %param.23) | copy-start | bytes 12292
  27.8 16.8 %all-to-all-start.2 = ((bf16[64,16,128]{2,0,1:T(8,128)(2,1)}), bf16[64,16,128]{2,0,1:T(8,128)(2,1)S(1)}, u32[]{:S(2)}, u32[]{:S(2)}) async-start(bf16[64,16,128]{2,0,1:T(8,128)(2,1)} %copy_bitcast_fusion), calls=%async_computation.2 | async-start | bytes 524288 | tf_op jit(solution)/shard_map/all_to_all | solution.py:132
  45.5 19.5 %all-to-all-start.1 = ((bf16[16,256,64]{1,2,0:T(8,128)(2,1)}), bf16[16,256,64]{1,2,0:T(8,128)(2,1)S(1)}, u32[]{:S(2)}, u32[]{:S(2)}) async-start(bf16[16,256,64]{1,2,0:T(8,128)(2,1)} %broadcast_in_dim.11), calls=%async_computation.1 | async-start | bytes 1048576 | tf_op jit(solution)/shard_map/all_to_all | solution.py:37
  66.0 12.0 %all-to-all-start.3 = ((f32[16,1,256]{2,1,0:T(1,128)}), f32[16,1,256]{2,1,0:T(1,128)S(1)}, u32[]{:S(2)}, u32[]{:S(2)}) async-start(f32[16,1,256]{2,1,0:T(1,128)} %broadcast_in_dim.12), calls=%async_computation.3 | async-start | bytes 32768 | tf_op jit(solution)/shard_map/all_to_all | solution.py:37
  79.2 29.6 %all-to-all-start.4 = ((bf16[16,256,128]{1,2,0:T(8,128)(2,1)}), bf16[16,256,128]{1,2,0:T(8,128)(2,1)S(1)}, u32[]{:S(2)}, u32[]{:S(2)}) async-start(bf16[16,256,128]{1,2,0:T(8,128)(2,1)} %broadcast_in_dim.13), calls=%async_computation.4 | async-start | bytes 2097152 | tf_op jit(solution)/shard_map/all_to_all | solution.py:37
  84.1 114.7 %all-gather.3.cloned.1.call-start = ((), (), s32[]{:S(2)}) async-start(), calls=%async_computation.7 | async-start | bytes 8912896 | tf_op jit(solution)/shard_map/all_gather | solution.py:158
  84.1 63.0 %copy-start.4 = (bf16[64,2048]{1,0:T(8,128)(2,1)S(1)}, bf16[64,2048]{1,0:T(8,128)(2,1)}, u32[]{:S(2)}) copy-start(bf16[64,2048]{1,0:T(8,128)(2,1)} %param.27) | copy-start | bytes 786436
  109.8 89.0 %copy-start.2 = (bf16[2,64,2048]{2,1,0:T(8,128)(2,1)S(1)}, bf16[2,64,2048]{2,1,0:T(8,128)(2,1)}, u32[]{:S(2)}) copy-start(bf16[2,64,2048]{2,1,0:T(8,128)(2,1)} %param.24) | copy-start | bytes 1572868
  146.8 106.7 %all-gather.5.cloned.1.call-start = ((), (), s32[]{:S(2)}) async-start(), calls=%async_computation.8 | async-start | bytes 5013504 | tf_op jit(solution)/shard_map/all_gather | solution.py:52
  148.8 55.9 %copy-start.8 = (bf16[2,64,2048]{2,1,0:T(8,128)(2,1)S(1)}, bf16[2,64,2048]{2,1,0:T(8,128)(2,1)}, u32[]{:S(2)}) copy-start(bf16[2,64,2048]{2,1,0:T(8,128)(2,1)} %param.25) | copy-start | bytes 1572868
  198.8 5.9 %copy-start.1 = (bf16[16,32,2,2,2048]{4,1,3,0,2:T(8,128)(2,1)S(1)}, bf16[16,32,2,2,2048]{4,1,3,0,2:T(8,128)(2,1)}, u32[]{:S(2)}) copy-start(bf16[16,32,2,2,2048]{4,1,3,0,2:T(8,128)(2,1)} %all-gather.3.cloned.1.call-done) | copy-start | bytes 25165828
  272.0 32.5 %copy-start.5 = (bf16[16,128,16]{1,2,0:T(8,128)(2,1)S(1)}, bf16[16,128,16]{1,2,0:T(8,128)(2,1)}, u32[]{:S(2)}) copy-start(bf16[16,128,16]{1,2,0:T(8,128)(2,1)} %get-tuple-element.5) | copy-start | bytes 196612
  272.0 32.8 %copy-start.3 = (bf16[1024,128]{1,0:T(8,128)(2,1)S(1)}, bf16[1024,128]{1,0:T(8,128)(2,1)}, u32[]{:S(2)}) copy-start(bf16[1024,128]{1,0:T(8,128)(2,1)} %param.29) | copy-start | bytes 786436
Sparse Core Ops, SparseCore 0:
  147.0 51.7 all-gather.2
  208.7 44.7 all-gather.4
where the time goes:
time: 315 us; the launch traced here: 314 us
  waiting for transfers between devices  147 us (47%)
  blocking collectives  61.5 us (20%)
  starting transfers between devices  35.4 us (11%)
  local copies, waits for them, and re-layouts  33.1 us (11%)
  matrix products  17.8 us (6%)
  between operations  14.5 us (5%)
  other arithmetic  4.01 us (1%)
    all_gather x1, waiting for transfers between devices, local(): piece_rows = lax.all_gather(arrived, 'tp', axis=0, tiled=True)  50 us
    all_gather x1, waiting for transfers between devices, gather_turned(): result = lax.all_gather(both, axis, axis=0, tiled=True)  44.9 us
    all_to_all x3, waiting for transfers between devices, from_everyone(): return lax.all_to_all(copies, axis, split_axis=0, concat_axis=0, tiled=True)  41.4 us
    all_to_all x1, blocking collectives, local(): lax.all_to_all(outgoing, 'sp', split_axis=0, concat_axis=0, tiled=True)  33.3 us
    all_to_all x1, blocking collectives, local(): lax.all_to_all(routed_total.astype(jnp.bfloat16), 'sp', split_axis=1, con...  28.2 us
    all_to_all x3, starting transfers between devices, from_everyone(): return lax.all_to_all(copies, axis, split_axis=0, concat_axis=0, tiled=True)  15.6 us
    split x2, local copies, waits for them, and re-layouts, gather_turned(): jnp.split(result, [sum(widths[:k]) for k in range(1, len(widths))], axis=1)  11.3 us
    all_to_all x1, waiting for transfers between devices, local(): lax.all_to_all(w_out, 'tp', split_axis=1, concat_axis=0, tiled=True)  9.24 us
  transfers between devices with their start and end apart: 9, of which 7 were waited for; matrix products, arithmetic and copies ran while one was open for 3% of the time, Pallas kernels for 0%

commit v1 on v0

--- a/solution.py
+++ b/solution.py
@@ -129,7 +129,10 @@
     d_dev = w_down.shape[2]
     all_heads = gathered_copies(attended, "tp", 1)
     w_cols, stream_cols = (
-        lax.all_to_all(w_out, "tp", split_axis=1, concat_axis=0, tiled=True),
+        jnp.concatenate(
+            lax.all_to_all(jnp.stack(jnp.split(w_out, lax.axis_size("tp"), axis=1)), "tp", 0, 0),
+            axis=0,
+        ),
         lax.all_to_all(stream, "tp", split_axis=1, concat_axis=0, tiled=True),
     )
     projected = jnp.dot(all_heads, w_cols, preferred_element_type=jnp.float32)

time: 315 us -> 333 us (1.057)
  local copies, waits for them, and re-layouts: 33.1 us -> 52.5 us
    unnamed x20 -> x35, local copies, waits for them, and re-layouts: 0.19 us -> 20 us
  transfers between devices with their start and end apart: 9 -> 9, of which waited for: 7 -> 6; matrix products, arithmetic and copies ran while one was open for 3% -> 9% of each run, Pallas kernels for 0% -> 0%
where the time goes in v1:
time: 333 us; the launch traced here: 331 us
  waiting for transfers between devices  146 us (44%)
  blocking collectives  61.4 us (18%)
  local copies, waits for them, and re-layouts  52.5 us (16%)
  starting transfers between devices  35.4 us (11%)
  matrix products  17.8 us (5%)
  between operations  14.5 us (4%)
  other arithmetic  4.01 us (1%)
    all_gather x1, waiting for transfers between devices, local(): piece_rows = lax.all_gather(arrived, 'tp', axis=0, tiled=True)  50 us
    all_gather x1, waiting for transfers between devices, gather_turned(): result = lax.all_gather(both, axis, axis=0, tiled=True)  44.9 us
    all_to_all x3, waiting for transfers between devices, from_everyone(): return lax.all_to_all(copies, axis, split_axis=0, concat_axis=0, tiled=True)  41.4 us
    all_to_all x1, blocking collectives, local(): lax.all_to_all(outgoing, 'sp', split_axis=0, concat_axis=0, tiled=True)  33.2 us
    all_to_all x1, blocking collectives, local(): lax.all_to_all(routed_total.astype(jnp.bfloat16), 'sp', split_axis=1, con...  28.2 us
    unnamed x35, local copies, waits for them, and re-layouts  20 us
    all_to_all x3, starting transfers between devices, from_everyone(): return lax.all_to_all(copies, axis, split_axis=0, concat_axis=0, tiled=True)  15.6 us
    split x2, local copies, waits for them, and re-layouts, gather_turned(): jnp.split(result, [sum(widths[:k]) for k in range(1, len(widths))], axis=1)  11.3 us
  transfers between devices with their start and end apart: 9, of which 6 were waited for; matrix products, arithmetic and copies ran while one was open for 9% of the time, Pallas kernels for 0%

profile of v1, /device:TPU:8, one launch (start us, length us, event | category | flops | bytes accessed | tf_op | source)
XLA Modules:
  0.0 331.2 jit_solution(11646071065068909664)
XLA Ops:
  6.5 1.5 copy_bitcast_fusion
  8.1 9.1 %all-to-all-start = ((bf16[16,16,128]{2,0,1:T(8,128)(2,1)}), bf16[16,16,128]{2,0,1:T(8,128)(2,1)S(1)}, u32[]{:S(2)}, u32[]{:S(2)}) async-start(bf16[16,16,128]{2,0,1:T(8,128)(2,1)} %copy_bitcast_fusion), calls=%async_computation | async-start | bytes 131072 | tf_op jit(solution)/shard_map/all_to_all | solution.py:136
  18.2 1.9 collective-permute-start
  20.1 1.3 collective-permute-start.1
  21.6 1.3 constant_dynamic-update-slice_fusion.15
  22.9 1.3 constant_dynamic-update-slice_fusion.14
  24.2 1.3 constant_dynamic-update-slice_fusion.13
  25.6 1.3 constant_dynamic-update-slice_fusion.12
  26.9 1.3 constant_dynamic-update-slice_fusion.11
  28.2 1.3 constant_dynamic-update-slice_fusion.10
  29.5 1.3 constant_dynamic-update-slice_fusion.9
  30.8 1.3 constant_dynamic-update-slice_fusion.8
  32.1 1.3 constant_dynamic-update-slice_fusion.7
  33.5 1.3 constant_dynamic-update-slice_fusion.6
  34.8 1.3 constant_dynamic-update-slice_fusion.5
  36.1 1.3 constant_dynamic-update-slice_fusion.4
  37.4 1.3 constant_dynamic-update-slice_fusion.3
  38.7 1.3 constant_dynamic-update-slice_fusion.2
  40.1 1.3 constant_dynamic-update-slice_fusion.1
  41.4 1.3 constant_dynamic-update-slice_fusion
  44.0 1.3 fusion.50
  45.4 7.2 %all-to-all-start.2 = ((bf16[16,64,128]{2,1,0:T(8,128)(2,1)}), bf16[16,64,128]{2,1,0:T(8,128)(2,1)S(1)}, u32[]{:S(2)}, u32[]{:S(2)}) async-start(bf16[16,64,128]{2,1,0:T(8,128)(2,1)} %constant_dynamic-update-slice_fusion), calls=%async_computation.2 | async-start | bytes 524288 | tf_op jit(solution)/shard_map/all_to_all | solution.py:133
  53.0 9.2 %all-to-all-done.2 = bf16[16,64,128]{2,1,0:T(8,128)(2,1)S(1)} async-done(((bf16[16,64,128]{2,1,0:T(8,128)(2,1)}), bf16[16,64,128]{2,1,0:T(8,128)(2,1)S(1)}, u32[]{:S(2)}, u32[]{:S(2)}) %all-to-all-start.2) | async-done | bytes 262176 | tf_op jit(solution)/shard_map/all_to_all | solution.py:133
  63.0 5.0 %all-to-all-start.1 = ((bf16[16,256,64]{1,2,0:T(8,128)(2,1)}), bf16[16,256,64]{1,2,0:T(8,128)(2,1)S(1)}, u32[]{:S(2)}, u32[]{:S(2)}) async-start(bf16[16,256,64]{1,2,0:T(8,128)(2,1)} %broadcast_in_dim.11), calls=%async_computation.1 | async-start | bytes 1048576 | tf_op jit(solution)/shard_map/all_to_all | solution.py:37
  68.2 14.4 %all-to-all-done.1 = bf16[16,256,64]{1,2,0:T(8,128)(2,1)S(1)} async-done(((bf16[16,256,64]{1,2,0:T(8,128)(2,1)}), bf16[16,256,64]{1,2,0:T(8,128)(2,1)S(1)}, u32[]{:S(2)}, u32[]{:S(2)}) %all-to-all-start.1) | async-done | bytes 524320 | tf_op jit(solution)/shard_map/all_to_all | solution.py:37
  83.5 5.7 %all-to-all-start.3 = ((f32[16,1,256]{2,1,0:T(1,128)}), f32[16,1,256]{2,1,0:T(1,128)S(1)}, u32[]{:S(2)}, u32[]{:S(2)}) async-start(f32[16,1,256]{2,1,0:T(1,128)} %broadcast_in_dim.12), calls=%async_computation.3 | async-start | bytes 32768 | tf_op jit(solution)/shard_map/all_to_all | solution.py:37
  89.9 5.5 %all-to-all-done.3 = f32[16,1,256]{2,1,0:T(1,128)S(1)} async-done(((f32[16,1,256]{2,1,0:T(1,128)}), f32[16,1,256]{2,1,0:T(1,128)S(1)}, u32[]{:S(2)}, u32[]{:S(2)}) %all-to-all-start.3) | async-done | bytes 16416 | tf_op jit(solution)/shard_map/all_to_all | solution.py:37
  95.6 1.1 broadcast_in_dim.13
  96.7 4.9 %all-to-all-start.4 = ((bf16[16,256,128]{1,2,0:T(8,128)(2,1)}), bf16[16,256,128]{1,2,0:T(8,128)(2,1)S(1)}, u32[]{:S(2)}, u32[]{:S(2)}) async-start(bf16[16,256,128]{1,2,0:T(8,128)(2,1)} %broadcast_in_dim.13), calls=%async_computation.4 | async-start | bytes 2097152 | tf_op jit(solution)/shard_map/all_to_all | solution.py:37
  102.2 1.4 select_reduce_fusion.1
  103.7 1.0 select_reduce_fusion
  104.7 21.5 %all-to-all-done.4 = bf16[16,256,128]{1,2,0:T(8,128)(2,1)S(1)} async-done(((bf16[16,256,128]{1,2,0:T(8,128)(2,1)}), bf16[16,256,128]{1,2,0:T(8,128)(2,1)S(1)}, u32[]{:S(2)}, u32[]{:S(2)}) %all-to-all-start.4) | async-done | bytes 1048608 | tf_op jit(solution)/shard_map/all_to_all | solution.py:37
  126.2 1.1 copy.136
  127.3 1.3 reshape_reshape.2
  128.6 1.2 convolution_convert_fusion
  129.9 33.2 %all_to_all.48 = bf16[32,4,2048]{2,1,0:T(4,128)(2,1)S(1)} all-to-all(bf16[32,4,2048]{2,1,0:T(4,128)(2,1)S(1)} %all_to_all.38), channel_id=1, replica_groups=mesh['sp'=32,'tp'=16] {'sp'}, dimensions={0} | all-to-all | bytes 1048576 | tf_op jit(solution)/shard_map/all_to_all | solution.py:159
  163.2 1.1 copy.137
  164.9 1.2 fusion.18
  166.2 50.0 %all-gather.3.cloned.1.call-done = bf16[16,32,2,2,2048]{4,1,3,0,2:T(8,128)(2,1)} async-done(((bf16[1,32,2,2,2048]{4,1,3,0,2:T(8,128)(2,1)}), bf16[16,32,2,2,2048]{4,1,3,0,2:T(8,128)(2,1)}) %all-gather.3.cloned.1.call-update) | async-done | bytes 8388624 | tf_op jit(solution)/shard_map/all_gather | solution.py:161
  216.3 5.8 %convolution_bitcast_fusion.1 = f32[64,16,32,2,2]{0,2,4,1,3:T(8,128)S(1)} fusion(bf16[16,32,2,2,2048]{4,1,3,0,2:T(8,128)(2,1)} %all-gather.3.cloned.1.call-done, bf16[2,64,2048]{2,1,0:T(8,128)(2,1)S(1)} %copy-done.2), kind=kOutput, calls=%fused_computation.6 | convolution fusion | flops 536870912 | bytes 9437184 | tf_op jit(solution)/shard_map/tsecd,efd->tsecf/dot_general | solution.py:162
  222.1 2.3 fusion.4
  226.1 44.9 %all-gather.5.cloned.1.call-done = bf16[1024,2304]{1,0:T(8,128)(2,1)} async-done(((bf16[64,2304]{1,0:T(8,128)(2,1)}), bf16[1024,2304]{1,0:T(8,128)(2,1)}) %all-gather.5.cloned.1.call-update) | async-done | bytes 4718608 | tf_op jit(solution)/shard_map/all_gather | solution.py:52
  271.0 4.8 %split.72 = bf16[1024,2048]{1,0:T(8,128)(2,1)} slice(bf16[1024,2304]{1,0:T(8,128)(2,1)} %all-gather.5.cloned.1.call-done), slice={[0:1024], [0:2048]} | slice | bytes 8388608 | tf_op jit(solution)/shard_map/split | solution.py:53
  275.8 6.5 %copy.141 = bf16[1024,2048]{0,1:T(8,128)(2,1)} copy(bf16[1024,2048]{1,0:T(8,128)(2,1)} %split.72) | data formatting | bytes 8388608 | tf_op jit(solution)/shard_map/split | solution.py:53
  282.3 7.2 %reshape.235 = bf16[1024,16,32,2,2]{0,4,3,2,1:T(2,128)(2,1)} reshape(bf16[1024,2048]{0,1:T(8,128)(2,1)} %copy.141) | data formatting | bytes 8388608 | tf_op jit(solution)/shard_map/reshape | solution.py:56
  289.5 3.6 %fusion.8 = bf16[16,32,2,2,128]{4,1,3,0,2:T(8,128)(2,1)S(1)} fusion(bf16[1024,16,32,2,2]{0,4,3,2,1:T(2,128)(2,1)} %reshape.235, bf16[2,1024,128]{2,1,0:T(8,128)(2,1)S(1)} %copy-done), kind=kOutput, calls=%fused_computation.9 | convolution fusion | flops 537133056 | bytes 5242880 | tf_op jit(solution)/shard_map/tsecf,efd->tsecd/dot_general | solution.py:175
  293.6 28.2 %all_to_all.49 = bf16[16,32,2,2,128]{4,3,0,2,1:T(2,128)(2,1)S(1)} all-to-all(bf16[16,32,2,2,128]{4,3,0,2,1:T(2,128)(2,1)S(1)} %copy.143), channel_id=1, replica_groups=mesh['sp'=32,'tp'=16] {'sp'}, dimensions={1} | all-to-all | bytes 1048576 | tf_op jit(solution)/shard_map/all_to_all | solution.py:181
  322.3 1.3 fusion.16
  (73 shorter events, 9.8 us)
Async XLA Ops:
  6.5 283.0 %copy-start = (bf16[2,1024,128]{2,1,0:T(8,128)(2,1)S(1)}, bf16[2,1024,128]{2,1,0:T(8,128)(2,1)}, u32[]{:S(2)}) copy-start(bf16[2,1024,128]{2,1,0:T(8,128)(2,1)} %param.26) | copy-start | bytes 1572868
  8.1 37.3 %all-to-all-start = ((bf16[16,16,128]{2,0,1:T(8,128)(2,1)}), bf16[16,16,128]{2,0,1:T(8,128)(2,1)S(1)}, u32[]{:S(2)}, u32[]{:S(2)}) async-start(bf16[16,16,128]{2,0,1:T(8,128)(2,1)} %copy_bitcast_fusion), calls=%async_computation | async-start | bytes 131072 | tf_op jit(solution)/shard_map/all_to_all | solution.py:136
  18.2 25.2 %collective-permute-start = (bf16[128,128]{1,0:T(8,128)(2,1)S(1)}, bf16[128,128]{1,0:T(8,128)(2,1)S(1)}, u32[]{:S(2)}, u32[]{:S(2)}) collective-permute-start(bf16[128,128]{1,0:T(8,128)(2,1)S(1)} %get-tuple-element.10), channel_id=1, source_target_pairs={{0,16},{16,32},{32,48},{48,64},{64,80},{80,96},{96,112},{112,128},... | collective-permute-start | bytes 98312 | tf_op jit(solution)/shard_map/ppermute | solution.py:23
  20.1 23.3 %collective-permute-start.1 = (bf16[128,128]{1,0:T(8,128)(2,1)S(1)}, bf16[128,128]{1,0:T(8,128)(2,1)S(1)}, u32[]{:S(2)}, u32[]{:S(2)}) collective-permute-start(bf16[128,128]{1,0:T(8,128)(2,1)S(1)} %get-tuple-element.11), channel_id=1, source_target_pairs={{16,0},{32,16},{48,32},{64,48},{80,64},{96,80},{112,96},{128,112},... | collective-permute-start | bytes 98312 | tf_op jit(solution)/shard_map/ppermute | solution.py:24
  45.3 56.3 %copy-start.6 = (s32[256,4]{0,1:T(4,128)S(1)}, s32[256,4]{0,1:T(4,128)}, u32[]{:S(2)}) copy-start(s32[256,4]{0,1:T(4,128)} %param.22) | copy-start | bytes 12292
  45.3 56.6 %copy-start.7 = (f32[256,4]{0,1:T(4,128)S(1)}, f32[256,4]{0,1:T(4,128)}, u32[]{:S(2)}) copy-start(f32[256,4]{0,1:T(4,128)} %param.23) | copy-start | bytes 12292
  45.4 16.8 %all-to-all-start.2 = ((bf16[16,64,128]{2,1,0:T(8,128)(2,1)}), bf16[16,64,128]{2,1,0:T(8,128)(2,1)S(1)}, u32[]{:S(2)}, u32[]{:S(2)}) async-start(bf16[16,64,128]{2,1,0:T(8,128)(2,1)} %constant_dynamic-update-slice_fusion), calls=%async_computation.2 | async-start | bytes 524288 | tf_op jit(solution)/shard_map/all_to_all | solution.py:133
  63.0 19.5 %all-to-all-start.1 = ((bf16[16,256,64]{1,2,0:T(8,128)(2,1)}), bf16[16,256,64]{1,2,0:T(8,128)(2,1)S(1)}, u32[]{:S(2)}, u32[]{:S(2)}) async-start(bf16[16,256,64]{1,2,0:T(8,128)(2,1)} %broadcast_in_dim.11), calls=%async_computation.1 | async-start | bytes 1048576 | tf_op jit(solution)/shard_map/all_to_all | solution.py:37
  83.5 12.0 %all-to-all-start.3 = ((f32[16,1,256]{2,1,0:T(1,128)}), f32[16,1,256]{2,1,0:T(1,128)S(1)}, u32[]{:S(2)}, u32[]{:S(2)}) async-start(f32[16,1,256]{2,1,0:T(1,128)} %broadcast_in_dim.12), calls=%async_computation.3 | async-start | bytes 32768 | tf_op jit(solution)/shard_map/all_to_all | solution.py:37
  96.7 29.6 %all-to-all-start.4 = ((bf16[16,256,128]{1,2,0:T(8,128)(2,1)}), bf16[16,256,128]{1,2,0:T(8,128)(2,1)S(1)}, u32[]{:S(2)}, u32[]{:S(2)}) async-start(bf16[16,256,128]{1,2,0:T(8,128)(2,1)} %broadcast_in_dim.13), calls=%async_computation.4 | async-start | bytes 2097152 | tf_op jit(solution)/shard_map/all_to_all | solution.py:37
  101.6 114.7 %all-gather.3.cloned.1.call-start = ((), (), s32[]{:S(2)}) async-start(), calls=%async_computation.7 | async-start | bytes 8912896 | tf_op jit(solution)/shard_map/all_gather | solution.py:161
  101.6 62.9 %copy-start.4 = (bf16[64,2048]{1,0:T(8,128)(2,1)S(1)}, bf16[64,2048]{1,0:T(8,128)(2,1)}, u32[]{:S(2)}) copy-start(bf16[64,2048]{1,0:T(8,128)(2,1)} %param.27) | copy-start | bytes 786436
  127.3 89.0 %copy-start.2 = (bf16[2,64,2048]{2,1,0:T(8,128)(2,1)S(1)}, bf16[2,64,2048]{2,1,0:T(8,128)(2,1)}, u32[]{:S(2)}) copy-start(bf16[2,64,2048]{2,1,0:T(8,128)(2,1)} %param.24) | copy-start | bytes 1572868
  164.3 106.7 %all-gather.5.cloned.1.call-start = ((), (), s32[]{:S(2)}) async-start(), calls=%async_computation.8 | async-start | bytes 5013504 | tf_op jit(solution)/shard_map/all_gather | solution.py:52
  166.2 55.9 %copy-start.8 = (bf16[2,64,2048]{2,1,0:T(8,128)(2,1)S(1)}, bf16[2,64,2048]{2,1,0:T(8,128)(2,1)}, u32[]{:S(2)}) copy-start(bf16[2,64,2048]{2,1,0:T(8,128)(2,1)} %param.25) | copy-start | bytes 1572868
  216.3 5.9 %copy-start.1 = (bf16[16,32,2,2,2048]{4,1,3,0,2:T(8,128)(2,1)S(1)}, bf16[16,32,2,2,2048]{4,1,3,0,2:T(8,128)(2,1)}, u32[]{:S(2)}) copy-start(bf16[16,32,2,2,2048]{4,1,3,0,2:T(8,128)(2,1)} %all-gather.3.cloned.1.call-done) | copy-start | bytes 25165828
  289.5 32.5 %copy-start.5 = (bf16[16,128,16]{1,2,0:T(8,128)(2,1)S(1)}, bf16[16,128,16]{1,2,0:T(8,128)(2,1)}, u32[]{:S(2)}) copy-start(bf16[16,128,16]{1,2,0:T(8,128)(2,1)} %get-tuple-element.5) | copy-start | bytes 196612
  289.5 32.8 %copy-start.3 = (bf16[1024,128]{1,0:T(8,128)(2,1)S(1)}, bf16[1024,128]{1,0:T(8,128)(2,1)}, u32[]{:S(2)}) copy-start(bf16[1024,128]{1,0:T(8,128)(2,1)} %param.29) | copy-start | bytes 786436
Sparse Core Ops, SparseCore 0:
  164.4 51.7 all-gather.2
  226.2 44.7 all-gather.4
